TPU v7x, 32 devices: a whole 2x2x4 slice. The times are simulated.
32 devices in a mesh: fs: 8 (over z, x), tp: 4 (over y, core).
Axes of the slice: x: 2, y: 2, z: 4, core: 2. Of those that a mesh axis runs over, the one named last changes fastest.
Arguments:
- inputs: bfloat16 [8192, 2048], P('fs'), may hold values from -6 to 6
- cotangents: bfloat16 [8192, 3, 1024], P('fs', None, 'tp'), may hold values from -0.06591797 to 0.06591797
- factors: bfloat16 [3, 2048, 256], P(None, 'fs'), may hold values from -13.810679 to 13.810679
- first_moment: float32 [3, 256, 1024], P(None, None, 'tp'), may hold values from -6 to 6
- second_moment: float32 [3, 256, 1024], P(None, None, 'tp'), may hold values from 0.05 to 1
- master: float32 [3, 2048, 1024], P(None, 'fs', 'tp'), may hold values from -0.125 to 0.125
Outputs:
- update_step: float32 [3, 2048, 1024], P(None, 'fs', 'tp')
- new_master: float32 [3, 2048, 1024], P(None, 'fs', 'tp')
- new_copy: bfloat16 [3, 2048, 1024], P(None, None, 'tp')
- new_first: float32 [3, 256, 1024], P(None, None, 'tp')
- new_second: float32 [3, 256, 1024], P(None, None, 'tp')
All inputs are finite; a program needn't handle non-finite values.
Results may differ from a plain program's by a relative error of at most 0.001.
Values may be sent and summed in bfloat16 or wider, within the bound.
A program may use at most 64 MiB of HBM per device.

v0:
```python
import jax
import jax.numpy as jnp
from jax import lax
from jax.sharding import PartitionSpec as P

D = 2048
MW = 1024
beta_first = 0.8
beta_second = 0.9
adam_eps = 1e-08
norm_eps = 1e-06
learning_rate = 0.005


def local(inputs, cotangents, factors, first_moment, second_moment, master):
    factor32 = factors.astype(jnp.float32)
    lowered = jnp.einsum(
        "tk,mkr->mtr",
        inputs,
        lax.all_gather(factors, "fs", axis=1, tiled=True),
        preferred_element_type=jnp.float32,
    )
    cot_wide = cotangents.astype(jnp.float32)
    partial_value = jnp.einsum("mtr,tmc->mrc", lowered, cot_wide, precision=lax.Precision.HIGHEST)
    projected = lax.psum(partial_value, "fs")
    new_first = beta_first * first_moment + (1.0 - beta_first) * projected
    new_second = beta_second * second_moment + (1.0 - beta_second) * projected * projected
    normed = new_first / (jnp.sqrt(new_second) + adam_eps)
    update = jnp.einsum("mdr,mrc->mdc", factor32, normed, precision=lax.Precision.HIGHEST)
    squares = lax.psum(jnp.sum(update * update, axis=(1, 2)), ("fs", "tp"))
    root_mean = jnp.sqrt(squares / (D * MW) + norm_eps)
    update_step = update / root_mean[:, None, None]
    new_master = master - learning_rate * update_step
    new_copy = lax.all_gather(new_master.astype(jnp.bfloat16), "fs", axis=1, tiled=True)
    return (update_step, new_master, new_copy, new_first, new_second)


def solution(mesh):
    placed = (
        P("fs", None),
        P("fs", None, "tp"),
        P(None, "fs", None),
        P(None, None, "tp"),
        P(None, None, "tp"),
        P(None, "fs", "tp"),
    )
    return jax.shard_map(
        local,
        mesh=mesh,
        in_specs=placed,
        out_specs=(
            P(None, "fs", "tp"),
            P(None, "fs", "tp"),
            P(None, None, "tp"),
            P(None, None, "tp"),
            P(None, None, "tp"),
        ),
        check_vma=False,
    )
```

profile of v0, /device:TPU:0, one launch (start us, length us, event | category | flops | bytes accessed | tf_op | source)
XLA Modules:
  0.0 275.3 jit_solution(5420966089030130023)
XLA Ops:
  7.2 0.0 copy-start
  7.2 0.0 all-gather.3.cloned.1.call-start
  7.2 0.7 all-gather.3.cloned.1.call-update
  7.9 0.0 all-reduce.2.cloned.1.call-start
  8.0 65.0 %all-gather.3.cloned.1.call-done = bf16[3,2048,256]{2,1,0:T(8,128)(2,1)} async-done(((bf16[3,256,256]{2,1,0:T(8,128)(2,1)}), bf16[3,2048,256]{2,1,0:T(8,128)(2,1)}) %all-gather.3.cloned.1.call-update) | async-done | bytes 3145744 | tf_op jit(solution)/shard_map/all_gather | solution.py:20
  72.9 6.2 %fusion = f32[3,256,1024]{2,1,0:T(8,128)S(1)} fusion(bf16[3,2048,256]{2,1,0:T(8,128)(2,1)} %all-gather.3.cloned.1.call-done, bf16[1024,2048]{1,0:T(8,128)(2,1)} %param.6), kind=kOutput, calls=%fused_computation | convolution fusion | flops 3221225472 | bytes 10485760 | tf_op jit(solution)/shard_map/tk,mkr->mtr/dot_general | solution.py:17
  79.2 0.0 copy-start.1
  79.2 2.5 fusion.10
  81.7 0.0 all-reduce.2.cloned.1.call-update
  81.7 0.0 all-gather.5.cloned.1.call-start
  81.8 0.3 copy.12
  82.0 73.5 %all-reduce.2.cloned.1.call-done = f32[3,256,256]{2,1,0:T(8,128)} async-done(((f32[3,256,256]{2,1,0:T(8,128)}), f32[3,256,256]{2,1,0:T(8,128)}) %all-reduce.2.cloned.1.call-update) | async-done | bytes 786448 | tf_op jit(solution)/shard_map/psum | solution.py:25
  155.6 1.8 fusion.2
  157.4 0.0 copy-start.2
  157.4 0.0 copy-start.3
  157.4 0.9 copy-done.2
  158.3 1.8 multiply_reduce_fusion
  160.1 39.4 %psum.15 = f32[3]{0:T(128)S(1)} all-reduce(f32[3]{0:T(128)S(1)} %get-tuple-element.15), channel_id=1, replica_groups=mesh['fs'=8,'tp'=4] {'fs','tp'}, use_global_device_ids=true, to_apply=%region_2.0 | all-reduce | flops 3 | bytes 24 | tf_op jit(solution)/shard_map/psum | solution.py:30
  199.6 2.4 fusion.9
  202.0 0.0 all-gather.5.cloned.1.call-update
  202.0 2.3 copy.14
  204.3 1.1 copy.13
  205.4 58.7 %all-gather.5.cloned.1.call-done = bf16[3,2048,256]{1,2,0:T(8,128)(2,1)} async-done(((bf16[3,256,256]{1,2,0:T(8,128)(2,1)}), bf16[3,2048,256]{1,2,0:T(8,128)(2,1)}) %all-gather.5.cloned.1.call-update) | async-done | bytes 3145744 | tf_op jit(solution)/shard_map/all_gather | solution.py:34
  264.2 4.6 %copy.15 = bf16[3,2048,256]{2,1,0:T(8,128)(2,1)} copy(bf16[3,2048,256]{1,2,0:T(8,128)(2,1)} %all-gather.5.cloned.1.call-done) | data formatting | bytes 6291456
  (6 shorter events, 0.0 us)
Async XLA Ops:
  7.2 72.0 %copy-start = (bf16[1024,3,256]{2,0,1:T(8,128)(2,1)S(1)}, bf16[1024,3,256]{2,0,1:T(8,128)(2,1)}, u32[]{:S(2)}) copy-start(bf16[1024,3,256]{2,0,1:T(8,128)(2,1)} %param.7) | copy-start | bytes 4718596
  7.2 65.8 %all-gather.3.cloned.1.call-start = ((), (), s32[]{:S(2)}) async-start(), calls=%async_computation | async-start | bytes 3538944 | tf_op jit(solution)/shard_map/all_gather | solution.py:20
  7.9 147.7 %all-reduce.2.cloned.1.call-start = ((), (), s32[]{:S(2)}) async-start(), calls=%async_computation.1 | async-start | bytes 1572864 | tf_op jit(solution)/shard_map/psum | solution.py:25
  79.2 2.6 copy-start.1
  81.7 76.6 %copy-start.4 = (bf16[3,256,256]{2,1,0:T(8,128)(2,1)S(1)}, bf16[3,256,256]{2,1,0:T(8,128)(2,1)}, u32[]{:S(2)}) copy-start(bf16[3,256,256]{2,1,0:T(8,128)(2,1)} %param.8) | copy-start | bytes 1179652
  81.7 182.5 %all-gather.5.cloned.1.call-start = ((), (), s32[]{:S(2)}) async-start(), calls=%async_computation.2 | async-start | bytes 3538944 | tf_op jit(solution)/shard_map/all_gather | solution.py:34
  157.4 0.9 copy-start.2
  157.4 2.7 copy-start.3
Sparse Core Ops, SparseCore 0:
  10.2 62.7 all-gather.2
  81.8 73.7 all-reduce.1
  202.1 62.0 all-gather.4
where the time goes:
time: 276 us; the launch traced here: 275 us
  waiting for transfers between devices  198 us (72%)
  blocking collectives  39.4 us (14%)
  between operations  13.8 us (5%)
  matrix products  10.5 us (4%)
  local copies, waits for them, and re-layouts  9.21 us (3%)
  other arithmetic  4.22 us (2%)
    psum x1, waiting for transfers between devices, local(): projected = lax.psum(partial_value, 'fs')  73.5 us
    all_gather x1, waiting for transfers between devices, local(): lax.all_gather(factors, 'fs', axis=1, tiled=True)  65 us
    all_gather x1, waiting for transfers between devices, local(): lax.all_gather(new_master.astype(jnp.bfloat16), 'fs', axis=1, tiled=True)  58.7 us
    psum x1, blocking collectives, local(): squares = lax.psum(jnp.sum(update * update, axis=(1, 2)), ('fs', 'tp'))  39.4 us
    unnamed x14, local copies, waits for them, and re-layouts  9.21 us
    dot_general x1, matrix products, local(): jnp.einsum('tk,mkr->mtr', inputs, lax.all_gather(factors, 'fs', axis=1, t...  6.22 us
  transfers between devices with their start and end apart: 3, of which 3 were waited for; matrix products, arithmetic and copies ran while one was open for 1% of the time, Pallas kernels for 0%

commit v1 on v0

--- a/solution.py
+++ b/solution.py
@@ -27,7 +27,7 @@
     new_second = beta_second * second_moment + (1.0 - beta_second) * projected * projected
     normed = new_first / (jnp.sqrt(new_second) + adam_eps)
     update = jnp.einsum("mdr,mrc->mdc", factor32, normed, precision=lax.Precision.HIGHEST)
-    squares = lax.psum(jnp.sum(update * update, axis=(1, 2)), ("fs", "tp"))
+    squares = lax.psum(lax.psum(jnp.sum(update * update, axis=(1, 2)), "tp"), "fs")
     root_mean = jnp.sqrt(squares / (D * MW) + norm_eps)
     update_step = update / root_mean[:, None, None]
     new_master = master - learning_rate * update_step

time: 276 us -> 260 us (0.942)
  blocking collectives: 39.4 us -> 25.2 us
    psum x1 -> x2, blocking collectives: 39.4 us -> 25.2 us  [the longest x1 19.6 us: local(): lax.psum(lax.psum(jnp.sum(update * update, axis=(1, 2)), 'tp'), 'fs')]
    unnamed x14 -> x16, local copies, waits for them, and re-layouts: 9.21 us -> 8.97 us
where the time goes in v1:
time: 260 us
  waiting for transfers between devices  198 us (76%)
  blocking collectives  25.2 us (10%)
  between operations  13.8 us (5%)
  matrix products  10.5 us (4%)
  local copies, waits for them, and re-layouts  8.97 us (3%)
  other arithmetic  3.97 us (2%)
    psum x1, waiting for transfers between devices, local(): projected = lax.psum(partial_value, 'fs')  73.8 us
    all_gather x1, waiting for transfers between devices, local(): lax.all_gather(factors, 'fs', axis=1, tiled=True)  65 us
    all_gather x1, waiting for transfers between devices, local(): lax.all_gather(new_master.astype(jnp.bfloat16), 'fs', axis=1, tiled=True)  58 us
    psum x1, blocking collectives, local(): lax.psum(lax.psum(jnp.sum(update * update, axis=(1, 2)), 'tp'), 'fs')  19.6 us
    unnamed x16, local copies, waits for them, and re-layouts  8.97 us
    dot_general x1, matrix products, local(): jnp.einsum('tk,mkr->mtr', inputs, lax.all_gather(factors, 'fs', axis=1, t...  6.22 us
    psum x1, blocking collectives, local(): lax.psum(jnp.sum(update * update, axis=(1, 2)), 'tp')  5.64 us
  transfers between devices with their start and end apart: 3, of which 3 were waited for; matrix products, arithmetic and copies ran while one was open for 1% of the time, Pallas kernels for 0%

profile of v1, /device:TPU:0, one launch (start us, length us, event | category | flops | bytes accessed | tf_op | source)
XLA Modules:
  0.0 260.1 jit_solution(15907734993542520646)
XLA Ops:
  7.2 0.0 copy-start
  7.2 0.0 all-gather.3.cloned.1.call-start
  7.2 0.7 all-gather.3.cloned.1.call-update
  7.9 0.0 all-reduce.2.cloned.1.call-start
  8.0 65.0 %all-gather.3.cloned.1.call-done = bf16[3,2048,256]{2,1,0:T(8,128)(2,1)} async-done(((bf16[3,256,256]{2,1,0:T(8,128)(2,1)}), bf16[3,2048,256]{2,1,0:T(8,128)(2,1)}) %all-gather.3.cloned.1.call-update) | async-done | bytes 3145744 | tf_op jit(solution)/shard_map/all_gather | solution.py:20
  72.9 6.2 %fusion = f32[3,256,1024]{2,1,0:T(8,128)S(1)} fusion(bf16[3,2048,256]{2,1,0:T(8,128)(2,1)} %all-gather.3.cloned.1.call-done, bf16[1024,2048]{1,0:T(8,128)(2,1)} %param.6), kind=kOutput, calls=%fused_computation | convolution fusion | flops 3221225472 | bytes 10485760 | tf_op jit(solution)/shard_map/tk,mkr->mtr/dot_general | solution.py:17
  79.2 2.5 fusion.10
  81.7 0.0 all-reduce.2.cloned.1.call-update
  81.7 0.0 all-gather.5.cloned.1.call-start
  81.8 73.8 %all-reduce.2.cloned.1.call-done = f32[3,256,256]{2,1,0:T(8,128)} async-done(((f32[3,256,256]{2,1,0:T(8,128)}), f32[3,256,256]{2,1,0:T(8,128)}) %all-reduce.2.cloned.1.call-update) | async-done | bytes 786448 | tf_op jit(solution)/shard_map/psum | solution.py:25
  155.6 1.6 fusion.2
  157.2 0.0 copy-start.3
  157.2 0.0 copy-start.4
  157.2 0.9 copy-done.3
  158.1 1.8 multiply_reduce_fusion
  159.9 5.6 %psum.22 = f32[3]{0:T(128)S(1)} all-reduce(f32[3]{0:T(128)S(1)} %get-tuple-element.15), channel_id=1, replica_groups=mesh['fs'=8,'tp'=4] {'tp'}, use_global_device_ids=true, to_apply=%region_2.0 | all-reduce | flops 3 | bytes 24 | tf_op jit(solution)/shard_map/psum | solution.py:30
  165.5 1.1 copy.12
  166.7 19.6 %psum.23 = f32[3]{0:T(128)S(1)} all-reduce(f32[3]{0:T(128)S(1)} %psum.22), channel_id=1, replica_groups=mesh['fs'=8,'tp'=4] {'fs'}, use_global_device_ids=true, to_apply=%region_3.0 | all-reduce | flops 3 | bytes 24 | tf_op jit(solution)/shard_map/psum | solution.py:30
  186.3 2.4 fusion.9
  188.6 0.0 all-gather.5.cloned.1.call-update
  188.7 1.1 copy.14
  189.8 1.1 copy.13
  191.0 58.0 %all-gather.5.cloned.1.call-done = bf16[3,2048,256]{1,2,0:T(8,128)(2,1)} async-done(((bf16[3,256,256]{1,2,0:T(8,128)(2,1)}), bf16[3,2048,256]{1,2,0:T(8,128)(2,1)}) %all-gather.5.cloned.1.call-update) | async-done | bytes 3145744 | tf_op jit(solution)/shard_map/all_gather | solution.py:34
  249.0 4.6 %copy.15 = bf16[3,2048,256]{2,1,0:T(8,128)(2,1)} copy(bf16[3,2048,256]{1,2,0:T(8,128)(2,1)} %all-gather.5.cloned.1.call-done) | data formatting | bytes 6291456
  (9 shorter events, 0.0 us)
Async XLA Ops:
  7.2 72.0 %copy-start = (bf16[1024,3,256]{2,0,1:T(8,128)(2,1)S(1)}, bf16[1024,3,256]{2,0,1:T(8,128)(2,1)}, u32[]{:S(2)}) copy-start(bf16[1024,3,256]{2,0,1:T(8,128)(2,1)} %param.7) | copy-start | bytes 4718596
  7.2 65.8 %all-gather.3.cloned.1.call-start = ((), (), s32[]{:S(2)}) async-start(), calls=%async_computation | async-start | bytes 3538944 | tf_op jit(solution)/shard_map/all_gather | solution.py:20
  7.9 147.7 %all-reduce.2.cloned.1.call-start = ((), (), s32[]{:S(2)}) async-start(), calls=%async_computation.1 | async-start | bytes 1572864 | tf_op jit(solution)/shard_map/psum | solution.py:25
  79.2 76.4 %copy-start.2 = (f32[3,256,256]{2,1,0:T(8,128)S(1)}, f32[3,256,256]{2,1,0:T(8,128)}, u32[]{:S(2)}) copy-start(f32[3,256,256]{2,1,0:T(8,128)} %param.10) | copy-start | bytes 2359300
  81.7 76.4 %copy-start.5 = (bf16[3,256,256]{2,1,0:T(8,128)(2,1)S(1)}, bf16[3,256,256]{2,1,0:T(8,128)(2,1)}, u32[]{:S(2)}) copy-start(bf16[3,256,256]{2,1,0:T(8,128)(2,1)} %param.8) | copy-start | bytes 1179652
  81.7 83.8 %copy-start.1 = (f32[3,256,256]{2,1,0:T(8,128)S(1)}, f32[3,256,256]{2,1,0:T(8,128)}, u32[]{:S(2)}) copy-start(f32[3,256,256]{2,1,0:T(8,128)} %param.11) | copy-start | bytes 2359300
  81.7 167.2 %all-gather.5.cloned.1.call-start = ((), (), s32[]{:S(2)}) async-start(), calls=%async_computation.2 | async-start | bytes 3538944 | tf_op jit(solution)/shard_map/all_gather | solution.py:34
  157.2 0.9 copy-start.3
  157.2 2.7 %copy-start.4 = (f32[3,256,256]{2,1,0:T(8,128)}, f32[3,256,256]{2,1,0:T(8,128)S(1)}, u32[]{:S(2)}) copy-start(f32[3,256,256]{2,1,0:T(8,128)S(1)} %get-tuple-element.14) | copy-start | bytes 2359300
Sparse Core Ops, SparseCore 0:
  10.2 62.7 all-gather.2
  81.8 73.7 all-reduce.1
  188.8 60.1 all-gather.4

commit v2 on v0

--- a/solution.py
+++ b/solution.py
@@ -22,7 +22,7 @@
     )
     cot_wide = cotangents.astype(jnp.float32)
     partial_value = jnp.einsum("mtr,tmc->mrc", lowered, cot_wide, precision=lax.Precision.HIGHEST)
-    projected = lax.psum(partial_value, "fs")
+    projected = jnp.sum(lax.all_gather(partial_value, "fs"), axis=0)
     new_first = beta_first * first_moment + (1.0 - beta_first) * projected
     new_second = beta_second * second_moment + (1.0 - beta_second) * projected * projected
     normed = new_first / (jnp.sqrt(new_second) + adam_eps)

time: 276 us -> 303 us (1.098)
  waiting for transfers between devices: 198 us -> 223 us
  other arithmetic: 4.22 us -> 7.33 us
    all_gather x0 -> x1, waiting for transfers between devices: none -> 97.2 us  [local(): projected = jnp.sum(lax.all_gather(partial_value, 'fs'), axis=0)]
    psum x1 -> x0, waiting for transfers between devices: 73.5 us -> none  [local(): projected = lax.psum(partial_value, 'fs')]
    reduce_sum x0 -> x1, other arithmetic: none -> 3.29 us  [local(): projected = jnp.sum(lax.all_gather(partial_value, 'fs'), axis=0)]
where the time goes in v2:
time: 303 us; the launch traced here: 302 us
  waiting for transfers between devices  223 us (74%)
  blocking collectives  38.3 us (13%)
  between operations  13.8 us (5%)
  matrix products  10.5 us (3%)
  local copies, waits for them, and re-layouts  9.21 us (3%)
  other arithmetic  7.33 us (2%)
    all_gather x1, waiting for transfers between devices, local(): projected = jnp.sum(lax.all_gather(partial_value, 'fs'), axis=0)  97.2 us
    all_gather x1, waiting for transfers between devices, local(): lax.all_gather(factors, 'fs', axis=1, tiled=True)  65 us
    all_gather x1, waiting for transfers between devices, local(): lax.all_gather(new_master.astype(jnp.bfloat16), 'fs', axis=1, tiled=True)  60.1 us
    psum x1, blocking collectives, local(): squares = lax.psum(jnp.sum(update * update, axis=(1, 2)), ('fs', 'tp'))  38.3 us
    unnamed x14, local copies, waits for them, and re-layouts  9.21 us
    dot_general x1, matrix products, local(): jnp.einsum('tk,mkr->mtr', inputs, lax.all_gather(factors, 'fs', axis=1, t...  6.22 us
  transfers between devices with their start and end apart: 3, of which 3 were waited for; matrix products, arithmetic and copies ran while one was open for 1% of the time, Pallas kernels for 0%

profile of v2, /device:TPU:0, one launch (start us, length us, event | category | flops | bytes accessed | tf_op | source)
XLA Modules:
  0.0 302.3 jit_solution(14630784286230721568)
XLA Ops:
  7.2 0.0 copy-start
  7.2 0.0 all-gather.5.cloned.1.call-start
  7.2 0.7 all-gather.5.cloned.1.call-update
  7.9 0.0 all-gather.9.cloned.1.call-start
  8.0 65.0 %all-gather.5.cloned.1.call-done = bf16[3,2048,256]{2,1,0:T(8,128)(2,1)} async-done(((bf16[3,256,256]{2,1,0:T(8,128)(2,1)}), bf16[3,2048,256]{2,1,0:T(8,128)(2,1)}) %all-gather.5.cloned.1.call-update) | async-done | bytes 3145744 | tf_op jit(solution)/shard_map/all_gather | solution.py:20
  72.9 6.2 %fusion = f32[3,256,1024]{2,1,0:T(8,128)S(1)} fusion(bf16[3,2048,256]{2,1,0:T(8,128)(2,1)} %all-gather.5.cloned.1.call-done, bf16[1024,2048]{1,0:T(8,128)(2,1)} %param.6), kind=kOutput, calls=%fused_computation | convolution fusion | flops 3221225472 | bytes 10485760 | tf_op jit(solution)/shard_map/tk,mkr->mtr/dot_general | solution.py:17
  79.2 2.5 fusion.10
  81.7 0.0 all-gather.9.cloned.1.call-update
  81.7 0.0 all-gather.7.cloned.1.call-start
  81.8 0.3 copy.17
  82.0 97.2 %all-gather.9.cloned.1.call-done = f32[24,256,256]{2,1,0:T(8,128)} async-done(((f32[3,256,256]{2,1,0:T(8,128)}), f32[24,256,256]{2,1,0:T(8,128)}) %all-gather.9.cloned.1.call-update) | async-done | bytes 6291472 | tf_op jit(solution)/shard_map/all_gather | solution.py:25
  179.2 3.3 %reduce_sum.18 = f32[3,256,256]{2,1,0:T(8,128)S(1)} reduce(f32[8,3,256,256]{3,2,1,0:T(8,128)} %bitcast.11, f32[]{:T(128)} %constant.2.clone.1), dimensions={0}, to_apply=%region_0.0 | reduce | flops 1376256 | bytes 7077892 | tf_op jit(solution)/shard_map/reduce_sum | solution.py:25
  182.5 1.6 fusion.2
  184.2 0.0 copy-start.2
  184.2 0.0 copy-start.3
  184.2 0.9 copy-done.2
  185.0 1.8 multiply_reduce_fusion
  186.9 38.3 %psum.7 = f32[3]{0:T(128)S(1)} all-reduce(f32[3]{0:T(128)S(1)} %get-tuple-element.20), channel_id=1, replica_groups=mesh['fs'=8,'tp'=4] {'fs','tp'}, use_global_device_ids=true, to_apply=%region_2.0 | all-reduce | flops 3 | bytes 24 | tf_op jit(solution)/shard_map/psum | solution.py:30
  225.2 2.4 fusion.9
  227.6 0.0 all-gather.7.cloned.1.call-update
  227.6 2.3 copy.19
  229.9 1.1 copy.18
  231.1 60.1 %all-gather.7.cloned.1.call-done = bf16[3,2048,256]{1,2,0:T(8,128)(2,1)} async-done(((bf16[3,256,256]{1,2,0:T(8,128)(2,1)}), bf16[3,2048,256]{1,2,0:T(8,128)(2,1)}) %all-gather.7.cloned.1.call-update) | async-done | bytes 3145744 | tf_op jit(solution)/shard_map/all_gather | solution.py:34
  291.1 4.6 %copy.20 = bf16[3,2048,256]{2,1,0:T(8,128)(2,1)} copy(bf16[3,2048,256]{1,2,0:T(8,128)(2,1)} %all-gather.7.cloned.1.call-done) | data formatting | bytes 6291456
  (7 shorter events, 0.0 us)
Async XLA Ops:
  7.2 72.0 %copy-start = (bf16[1024,3,256]{2,0,1:T(8,128)(2,1)S(1)}, bf16[1024,3,256]{2,0,1:T(8,128)(2,1)}, u32[]{:S(2)}) copy-start(bf16[1024,3,256]{2,0,1:T(8,128)(2,1)} %param.7) | copy-start | bytes 4718596
  7.2 65.8 %all-gather.5.cloned.1.call-start = ((), (), s32[]{:S(2)}) async-start(), calls=%async_computation | async-start | bytes 3538944 | tf_op jit(solution)/shard_map/all_gather | solution.py:20
  7.9 171.3 %all-gather.9.cloned.1.call-start = ((), (), s32[]{:S(2)}) async-start(), calls=%async_computation.2 | async-start | bytes 7077888 | tf_op jit(solution)/shard_map/all_gather | solution.py:25
  79.2 2.6 copy-start.1
  81.7 209.5 %all-gather.7.cloned.1.call-start = ((), (), s32[]{:S(2)}) async-start(), calls=%async_computation.1 | async-start | bytes 3538944 | tf_op jit(solution)/shard_map/all_gather | solution.py:34
  182.5 2.5 copy-start.4
  184.2 0.9 copy-start.2
  184.2 2.7 copy-start.3
Sparse Core Ops, SparseCore 0:
  10.2 62.7 all-gather.4
  81.8 97.3 all-gather.8
  227.8 63.3 all-gather.6
